TPU v7x, 128 devices: a whole 4x4x4 slice. The times are simulated.
128 devices in a mesh: fs: 32 (over z, y, core), tp: 4 (over x).
Axes of the slice: x: 4, y: 4, z: 4, core: 2. Of those that a mesh axis runs over, the one named last changes fastest.
Arguments:
- x_saved: bfloat16 [65536, 2048], P('fs'), may hold values from -6 to 6
- h_saved: bfloat16 [65536, 1024], P('fs', 'tp'), may hold values from -6 to 6
- key_cot: bfloat16 [65536, 1024], P('fs', 'tp'), may hold values from -6 to 6
- value_cot: bfloat16 [65536, 1024], P('fs', 'tp'), may hold values from -6 to 6
- out_cot: bfloat16 [65536, 2048], P('fs'), may hold values from -6 to 6
- w_key: float32 [2048, 1024], P('fs', 'tp'), may hold values from -0.125 to 0.125
- w_value: float32 [2048, 1024], P('fs', 'tp'), may hold values from -0.125 to 0.125
- w_out: float32 [1024, 2048], P('tp', 'fs'), may hold values from -0.1875 to 0.1875
- p_key: bfloat16 [2048, 256], P('fs'), may hold values from -1 to 1, as said below
- p_value: bfloat16 [2048, 256], P('fs'), may hold values from -1 to 1, as said below
- p_out: bfloat16 [2048, 256], P('fs'), may hold values from -1 to 1, as said below
- m_key: float32 [2, 256, 1024], P(None, 'fs', 'tp'), may hold values from -1.5 to 1.5, as said below
- m_value: float32 [2, 256, 1024], P(None, 'fs', 'tp'), may hold values from -1.5 to 1.5, as said below
- m_out: float32 [2, 256, 1024], P(None, 'fs', 'tp'), may hold values from -1.5 to 1.5, as said below
Outputs:
- step_key: float32 [2048, 1024], P('fs', 'tp')
- step_value: float32 [2048, 1024], P('fs', 'tp')
- step_out: float32 [1024, 2048], P('tp', 'fs')
- copy_key: bfloat16 [2048, 1024], P(None, 'tp')
- copy_value: bfloat16 [2048, 1024], P(None, 'tp')
- copy_out: bfloat16 [1024, 2048], P('tp')
- new_m_key: float32 [2, 256, 1024], P(None, 'fs', 'tp')
- new_m_value: float32 [2, 256, 1024], P(None, 'fs', 'tp')
- new_m_out: float32 [2, 256, 1024], P(None, 'fs', 'tp')
Inputs may be any that keep to these rules, and one draw needn't show every extreme that they name: `p_key`: factor entries are real-valued, dense and of full rank. `p_value`: factor entries are real-valued, dense and of full rank. `p_out`: factor entries are real-valued, dense and of full rank. `m_key`: plane 1 (second moments) lies in 0.05 to 1. `m_value`: plane 1 (second moments) lies in 0.05 to 1. `m_out`: plane 1 (second moments) lies in 0.05 to 1.
All inputs are finite; a program needn't handle non-finite values.
Results may differ from a plain program's by a relative error of at most 0.0085.
Values may be sent and summed in bfloat16 or wider, within the bound.
A program may use at most 128 MiB of HBM per device.

v0:
```python
import jax
import jax.numpy as jnp
from jax import lax
from jax.sharding import Mesh
from jax.sharding import PartitionSpec as P

FS = ("fs_0", "fs_1", "fs_2")


beta_one = 0.9
beta_two = 0.9
learn_rate = 0.01


def copy_for_each(value, axis):
    copies = jnp.broadcast_to(value, (lax.axis_size(axis), *value.shape))
    return lax.all_to_all(copies, axis, split_axis=0, concat_axis=0, tiled=True)


def joined_along(parts, dim):
    parts = jnp.moveaxis(parts, 0, dim)
    dims = parts.shape
    return parts.reshape(*dims[:dim], dims[dim] * dims[dim + 1], *dims[dim + 2 :])


def whole_of(value, axes, dim):
    far, near = axes
    first = copy_for_each(value, far)
    parts = jnp.swapaxes(copy_for_each(first, near), 0, 1)
    return joined_along(parts.reshape(-1, *value.shape), dim)


def in_one_piece(arrays, axis, dim, along):
    widths = [a.shape[along] for a in arrays]
    both = jnp.concatenate(arrays, axis=along)
    whole = whole_of(both, axis, dim)
    return tuple(jnp.split(whole, [sum(widths[:k]) for k in range(1, len(widths))], axis=along))


def in_blocks(value, dim, devices):
    dims = value.shape
    parts = value.reshape(*dims[:dim], devices, dims[dim] // devices, *dims[dim + 1 :])
    return jnp.moveaxis(parts, dim, 0)


def sent_and_summed(value, axis, dim):
    devices = lax.axis_size(axis)
    parts = lax.all_to_all(in_blocks(value, dim, devices), axis, 0, 0, tiled=True)
    return jnp.sum(parts.astype(jnp.float32), axis=0)


def over_copies(value, axis):
    return copy_for_each(value, axis).sum(axis=0)


def over_axes(value, axes):
    far, near = axes
    return over_copies(over_copies(value, near), far)


def gathered_copies(value, axis, dim):
    return joined_along(copy_for_each(value, axis), dim)


def project_rows(factors, grads, local_width):
    high_part = grads.astype(jnp.bfloat16)
    low_part = (grads - high_part.astype(jnp.float32)).astype(jnp.bfloat16)
    outputs = []
    for member in range(3):
        lower = member * local_width
        upper = (member + 1) * local_width
        factor_t = factors[member].T
        first_term = jnp.dot(
            factor_t, high_part[:, lower:upper], preferred_element_type=jnp.float32
        )
        second_term = jnp.dot(
            factor_t, low_part[:, lower:upper], preferred_element_type=jnp.float32
        )
        outputs.append(first_term + second_term)
    return jnp.concatenate(outputs, axis=1)


def body(
    x_saved,
    h_saved,
    key_cot,
    value_cot,
    out_cot,
    w_key,
    w_value,
    w_out,
    p_key,
    p_value,
    p_out,
    m_key,
    m_value,
    m_out,
):
    local_width = key_cot.shape[1]
    x_cols = x_saved.T
    y_cols = out_cot.T
    grad_k = jnp.dot(x_cols, key_cot, preferred_element_type=jnp.float32)
    grad_v = jnp.dot(x_cols, value_cot, preferred_element_type=jnp.float32)
    grad_o = jnp.dot(y_cols, h_saved, preferred_element_type=jnp.float32)
    whole_grad = jnp.concatenate([grad_k, grad_v, grad_o], axis=1)
    partial_value = project_rows(
        in_one_piece((p_key, p_value, p_out), (("fs_0", "fs_1"), "fs_2"), 0, 1),
        whole_grad,
        local_width,
    )
    projected = sent_and_summed(partial_value.astype(jnp.bfloat16), FS, 0)
    total = over_axes(jnp.sum(projected * projected), (("fs_0", "fs_1"), ("fs_2", "tp")))
    entries = projected.size * lax.axis_size(FS) * lax.axis_size("tp")
    normed = projected / jnp.sqrt(total / entries + 1e-06)
    moments = jnp.concatenate([m_key, m_value, m_out], axis=2)
    moment_one = beta_one * moments[0] + (1 - beta_one) * normed
    moment_two = beta_two * moments[1] + (1 - beta_two) * normed * normed
    direction = (moment_one / jnp.sqrt(moment_two)).astype(jnp.bfloat16)
    gathered = gathered_copies(direction, FS, 0)
    step_key = jnp.dot(p_key, gathered[:, :local_width], preferred_element_type=jnp.float32)
    step_value = jnp.dot(
        p_value, gathered[:, local_width : 2 * local_width], preferred_element_type=jnp.float32
    )
    step_out = jnp.dot(p_out, gathered[:, 2 * local_width :], preferred_element_type=jnp.float32).T
    fresh_key = (w_key - learn_rate * step_key).astype(jnp.bfloat16)
    fresh_value = (w_value - learn_rate * step_value).astype(jnp.bfloat16)
    fresh_out = (w_out - learn_rate * step_out).astype(jnp.bfloat16)
    copy_key, copy_value, copy_out = (
        *in_one_piece((fresh_key, fresh_value), (("fs_0", "fs_1"), "fs_2"), 0, 1),
        whole_of(fresh_out, (("fs_0", "fs_1"), "fs_2"), 1),
    )
    stacked = jnp.stack([moment_one, moment_two])
    new_m_key = stacked[:, :, :local_width]
    new_m_value = stacked[:, :, local_width : 2 * local_width]
    new_m_out = stacked[:, :, 2 * local_width :]
    return (
        step_key,
        step_value,
        step_out,
        copy_key,
        copy_value,
        copy_out,
        new_m_key,
        new_m_value,
        new_m_out,
    )


def solution(mesh):
    split = Mesh(mesh.devices.reshape(4, 4, 2, mesh.shape["tp"]), ("fs_0", "fs_1", "fs_2", "tp"))
    in_specs = (
        P(FS, None),
        P(FS, "tp"),
        P(FS, "tp"),
        P(FS, "tp"),
        P(FS, None),
        P(FS, "tp"),
        P(FS, "tp"),
        P("tp", FS),
        P(FS, None),
        P(FS, None),
        P(FS, None),
        P(None, FS, "tp"),
        P(None, FS, "tp"),
        P(None, FS, "tp"),
    )
    out_specs = (
        P(FS, "tp"),
        P(FS, "tp"),
        P("tp", FS),
        P(None, "tp"),
        P(None, "tp"),
        P("tp", None),
        P(None, FS, "tp"),
        P(None, FS, "tp"),
        P(None, FS, "tp"),
    )
    return jax.shard_map(body, mesh=split, in_specs=in_specs, out_specs=out_specs, check_vma=False)
```

profile of v0, /device:TPU:1, one launch (start us, length us, event | category | flops | bytes accessed | tf_op | source)
XLA Modules:
  0.0 154.7 jit_solution(2395847541230072677)
XLA Ops:
  0.7 0.9 pad_maximum_fusion.2
  1.5 1.3 broadcast_in_dim.27
  2.9 8.6 %all-to-all-start = ((bf16[16,64,768]{2,1,0:T(8,128)(2,1)}), bf16[16,64,768]{2,1,0:T(8,128)(2,1)S(1)}, u32[]{:S(2)}, u32[]{:S(2)}) async-start(bf16[16,64,768]{2,1,0:T(8,128)(2,1)} %broadcast_in_dim.27), calls=%async_computation | async-start | bytes 3145728 | tf_op jit(solution)/shard_map/all_to_all | solution.py:17
  11.5 5.9 %fusion.34 = f32[2048,256]{0,1:T(8,128)S(1)} fusion(bf16[2048,2048]{1,0:T(8,128)(2,1)} %param.14, bf16[2048,256]{1,0:T(8,128)(2,1)S(1)} %copy-done), kind=kOutput, calls=%fused_computation.64 | convolution fusion | flops 2147483648 | bytes 11534336 | tf_op jit(solution)/shard_map/dot_general | solution.py:102
  17.4 5.9 %fusion.35 = f32[2048,256]{0,1:T(8,128)S(1)} fusion(bf16[2048,2048]{1,0:T(8,128)(2,1)} %param.14, bf16[2048,256]{1,0:T(8,128)(2,1)S(1)} %copy-done.12), kind=kOutput, calls=%fused_computation.65 | convolution fusion | flops 2147483648 | bytes 11534336 | tf_op jit(solution)/shard_map/dot_general | solution.py:103
  23.4 2.4 %fusion.36 = f32[2048,256]{0,1:T(8,128)S(1)} fusion(bf16[2048,2048]{1,0:T(8,128)(2,1)S(1)} %bitcast.52, bf16[2048,256]{1,0:T(8,128)(2,1)S(1)} %copy-done.13), kind=kOutput, calls=%fused_computation.66 | convolution fusion | flops 2147483648 | bytes 11534336 | tf_op jit(solution)/shard_map/dot_general | solution.py:104
  25.8 2.1 %subtract_convert_fusion = bf16[2048,768]{0,1:T(8,128)(2,1)} fusion(f32[2048,256]{0,1:T(8,128)S(1)} %fusion.36, f32[2048,256]{0,1:T(8,128)S(1)} %fusion.35, f32[2048,256]{0,1:T(8,128)S(1)} %fusion.34), kind=kLoop, calls=%fused_computation.1 | loop fusion | flops 9437184 | bytes 9437184 | tf_op jit(solution)/shard_map/convert_element_type | solution.py:67
  27.8 2.0 %fusion = bf16[2048,768]{0,1:T(8,128)(2,1)} fusion(f32[2048,256]{0,1:T(8,128)S(1)} %fusion.36, f32[2048,256]{0,1:T(8,128)S(1)} %fusion.35, f32[2048,256]{0,1:T(8,128)S(1)} %fusion.34), kind=kLoop, calls=%fused_computation.2 | loop fusion | flops 9437184 | bytes 9437184 | tf_op jit(solution)/shard_map/convert_element_type | solution.py:66
  29.8 4.7 %all-to-all-done = bf16[16,64,768]{2,1,0:T(8,128)(2,1)S(1)} async-done(((bf16[16,64,768]{2,1,0:T(8,128)(2,1)}), bf16[16,64,768]{2,1,0:T(8,128)(2,1)S(1)}, u32[]{:S(2)}, u32[]{:S(2)}) %all-to-all-start) | async-done | bytes 1572896 | tf_op jit(solution)/shard_map/all_to_all | solution.py:17
  35.0 8.3 %all_to_all.52 = bf16[2,16,64,768]{3,2,1,0:T(8,128)(2,1)S(1)} all-to-all(bf16[2,16,64,768]{3,2,1,0:T(8,128)(2,1)S(1)} %broadcast_in_dim.28), channel_id=1, replica_groups=mesh['fs_0'=4,'fs_1'=4,'fs_2'=2,'tp'=4] {'fs_2'}, dimensions={0} | all-to-all | bytes 6291456 | tf_op jit(solution)/shard_map/all_to_all | solution.py:17
  43.6 1.6 %copy-done.2 = bf16[2048,768]{0,1:T(8,128)(2,1)S(1)} copy-done((bf16[2048,768]{0,1:T(8,128)(2,1)S(1)}, bf16[2048,768]{0,1:T(8,128)(2,1)}, u32[]{:S(2)}) %copy-start.2) | copy-done | bytes 3145752
  46.6 0.9 copy-done.1
  49.9 3.9 %all-to-all-start.2 = ((bf16[32,8,768]{2,1,0:T(8,128)(2,1)}), bf16[32,8,768]{2,1,0:T(8,128)(2,1)S(1)}, u32[]{:S(2)}, u32[]{:S(2)}) async-start(bf16[32,8,768]{2,1,0:T(8,128)(2,1)} %pad_maximum_fusion.1), calls=%async_computation.2 | async-start | bytes 786432 | tf_op jit(solution)/shard_map/all_to_all | solution.py:48
  53.8 10.2 %all-to-all-done.2 = bf16[32,8,768]{2,1,0:T(8,128)(2,1)S(1)} async-done(((bf16[32,8,768]{2,1,0:T(8,128)(2,1)}), bf16[32,8,768]{2,1,0:T(8,128)(2,1)S(1)}, u32[]{:S(2)}, u32[]{:S(2)}) %all-to-all-start.2) | async-done | bytes 393248 | tf_op jit(solution)/shard_map/all_to_all | solution.py:48
  65.3 9.0 %all_to_all.53 = f32[8,1,1]{2,1,0:T(1,128)S(1)} all-to-all(f32[8,1,1]{2,1,0:T(1,128)S(1)} %broadcast_in_dim.29), channel_id=1, replica_groups=mesh['fs_0'=4,'fs_1'=4,'fs_2'=2,'tp'=4] {'fs_2','tp'}, dimensions={0} | all-to-all | bytes 64 | tf_op jit(solution)/shard_map/all_to_all | solution.py:17
  74.9 1.2 broadcast_in_dim.30
  76.2 3.5 %all-to-all-start.4 = ((f32[16,1,1]{2,1,0:T(1,128)}), f32[16,1,1]{2,1,0:T(1,128)S(1)}, u32[]{:S(2)}, u32[]{:S(2)}) async-start(f32[16,1,1]{2,1,0:T(1,128)} %broadcast_in_dim.30), calls=%async_computation.4 | async-start | bytes 16384 | tf_op jit(solution)/shard_map/all_to_all | solution.py:17
  79.7 6.3 %all-to-all-done.4 = f32[16,1,1]{2,1,0:T(1,128)S(1)} async-done(((f32[16,1,1]{2,1,0:T(1,128)}), f32[16,1,1]{2,1,0:T(1,128)S(1)}, u32[]{:S(2)}, u32[]{:S(2)}) %all-to-all-start.4) | async-done | bytes 96 | tf_op jit(solution)/shard_map/all_to_all | solution.py:17
  87.3 15.0 %all_to_all.54 = bf16[32,8,768]{2,1,0:T(8,128)(2,1)S(1)} all-to-all(bf16[32,8,768]{2,1,0:T(8,128)(2,1)S(1)} %broadcast_in_dim.31), channel_id=1, replica_groups=mesh['fs_0'=4,'fs_1'=4,'fs_2'=2,'tp'=4] {'fs_0','fs_1','fs_2'}, dimensions={0} | all-to-all | bytes 786432 | tf_op jit(solution)/shard_map/all_to_all | solution.py:17
  102.4 0.8 subtract_convert_fusion.1
  103.2 0.8 broadcast_in_dim.34
  104.0 3.6 %all-to-all-start.8 = ((bf16[16,256,64]{1,2,0:T(8,128)(2,1)}), bf16[16,256,64]{1,2,0:T(8,128)(2,1)S(1)}, u32[]{:S(2)}, u32[]{:S(2)}) async-start(bf16[16,256,64]{1,2,0:T(8,128)(2,1)} %broadcast_in_dim.34), calls=%async_computation.8 | async-start | bytes 1048576 | tf_op jit(solution)/shard_map/all_to_all | solution.py:17
  107.6 0.8 subtract_convert_fusion.2
  109.2 9.4 %all-to-all-done.8 = bf16[16,256,64]{1,2,0:T(8,128)(2,1)S(1)} async-done(((bf16[16,256,64]{1,2,0:T(8,128)(2,1)}), bf16[16,256,64]{1,2,0:T(8,128)(2,1)S(1)}, u32[]{:S(2)}, u32[]{:S(2)}) %all-to-all-start.8) | async-done | bytes 524320 | tf_op jit(solution)/shard_map/all_to_all | solution.py:17
  118.7 5.6 %all_to_all.55 = bf16[2,16,256,64]{2,3,1,0:T(8,128)(2,1)S(1)} all-to-all(bf16[2,16,256,64]{2,3,1,0:T(8,128)(2,1)S(1)} %broadcast_in_dim.35), channel_id=1, replica_groups=mesh['fs_0'=4,'fs_1'=4,'fs_2'=2,'tp'=4] {'fs_2'}, dimensions={0} | all-to-all | bytes 2097152 | tf_op jit(solution)/shard_map/all_to_all | solution.py:17
  124.4 1.1 broadcast_in_dim.32
  125.4 3.7 %all-to-all-start.6 = ((bf16[16,64,512]{2,1,0:T(8,128)(2,1)}), bf16[16,64,512]{2,1,0:T(8,128)(2,1)S(1)}, u32[]{:S(2)}, u32[]{:S(2)}) async-start(bf16[16,64,512]{2,1,0:T(8,128)(2,1)} %broadcast_in_dim.32), calls=%async_computation.6 | async-start | bytes 2097152 | tf_op jit(solution)/shard_map/all_to_all | solution.py:17
  129.7 1.0 copy.40
  130.8 2.3 %copy.41 = bf16[256,2048]{1,0:T(8,128)(2,1)} copy(bf16[256,2048]{0,1:T(8,128)(2,1)} %bitcast.41) | data formatting | bytes 2097152
  133.0 12.9 %all-to-all-done.6 = bf16[16,64,512]{2,1,0:T(8,128)(2,1)S(1)} async-done(((bf16[16,64,512]{2,1,0:T(8,128)(2,1)}), bf16[16,64,512]{2,1,0:T(8,128)(2,1)S(1)}, u32[]{:S(2)}, u32[]{:S(2)}) %all-to-all-start.6) | async-done | bytes 1048608 | tf_op jit(solution)/shard_map/all_to_all | solution.py:17
  146.2 6.9 %all_to_all.56 = bf16[2,16,64,512]{3,2,1,0:T(8,128)(2,1)S(1)} all-to-all(bf16[2,16,64,512]{3,2,1,0:T(8,128)(2,1)S(1)} %broadcast_in_dim.33), channel_id=1, replica_groups=mesh['fs_0'=4,'fs_1'=4,'fs_2'=2,'tp'=4] {'fs_2'}, dimensions={0} | all-to-all | bytes 4194304 | tf_op jit(solution)/shard_map/all_to_all | solution.py:17
  153.3 1.5 fusion.33
  (57 shorter events, 9.1 us)
Async XLA Ops:
  0.6 10.8 %copy-start = (bf16[2048,256]{1,0:T(8,128)(2,1)S(1)}, bf16[2048,256]{1,0:T(8,128)(2,1)}, u32[]{:S(2)}) copy-start(bf16[2048,256]{1,0:T(8,128)(2,1)} %param.16) | copy-start | bytes 3145732
  2.9 31.7 %all-to-all-start = ((bf16[16,64,768]{2,1,0:T(8,128)(2,1)}), bf16[16,64,768]{2,1,0:T(8,128)(2,1)S(1)}, u32[]{:S(2)}, u32[]{:S(2)}) async-start(bf16[16,64,768]{2,1,0:T(8,128)(2,1)} %broadcast_in_dim.27), calls=%async_computation | async-start | bytes 3145728 | tf_op jit(solution)/shard_map/all_to_all | solution.py:17
  11.5 5.9 %copy-start.12 = (bf16[2048,256]{1,0:T(8,128)(2,1)S(1)}, bf16[2048,256]{1,0:T(8,128)(2,1)}, u32[]{:S(2)}) copy-start(bf16[2048,256]{1,0:T(8,128)(2,1)} %param.17) | copy-start | bytes 3145732
  11.5 11.9 %slice-start = ((s8[8388608]{0:T(1024)(128)(4,1)}), s8[4194304]{0:T(1024)(128)(4,1)S(1)}, s32[]{:S(2)}) async-start(s8[8388608]{0:T(1024)(128)(4,1)} %bitcast.51), calls=%async_computation.10 | async-start | bytes 8388608
  17.4 5.9 %slice-start.1 = ((s8[8388608]{0:T(1024)(128)(4,1)}), s8[4194304]{0:T(1024)(128)(4,1)S(1)}, s32[]{:S(2)}) async-start(s8[8388608]{0:T(1024)(128)(4,1)} %bitcast.51), calls=%async_computation.11 | async-start | bytes 8388608
  17.4 5.9 %copy-start.13 = (bf16[2048,256]{1,0:T(8,128)(2,1)S(1)}, bf16[2048,256]{1,0:T(8,128)(2,1)}, u32[]{:S(2)}) copy-start(bf16[2048,256]{1,0:T(8,128)(2,1)} %param.15) | copy-start | bytes 3145732
  43.2 1.9 %copy-start.2 = (bf16[2048,768]{0,1:T(8,128)(2,1)S(1)}, bf16[2048,768]{0,1:T(8,128)(2,1)}, u32[]{:S(2)}) copy-start(bf16[2048,768]{0,1:T(8,128)(2,1)} %fusion) | copy-start | bytes 9437188
  45.6 1.9 %copy-start.1 = (bf16[2048,768]{0,1:T(8,128)(2,1)S(1)}, bf16[2048,768]{0,1:T(8,128)(2,1)}, u32[]{:S(2)}) copy-start(bf16[2048,768]{0,1:T(8,128)(2,1)} %subtract_convert_fusion) | copy-start | bytes 9437188
  48.5 5.3 %copy-start.9 = (f32[2,8,256]{2,1,0:T(8,128)S(1)}, f32[2,8,256]{2,1,0:T(8,128)}, u32[]{:S(2)}) copy-start(f32[2,8,256]{2,1,0:T(8,128)} %param.25) | copy-start | bytes 49156
  48.5 5.3 %copy-start.10 = (f32[2,8,256]{2,1,0:T(8,128)S(1)}, f32[2,8,256]{2,1,0:T(8,128)}, u32[]{:S(2)}) copy-start(f32[2,8,256]{2,1,0:T(8,128)} %param.26) | copy-start | bytes 49156
  48.5 31.2 %copy-start.11 = (f32[2,8,256]{2,1,0:T(8,128)S(1)}, f32[2,8,256]{2,1,0:T(8,128)}, u32[]{:S(2)}) copy-start(f32[2,8,256]{2,1,0:T(8,128)} %param.27) | copy-start | bytes 49156
  48.5 53.9 %copy-start.3 = (bf16[64,256]{1,0:T(8,128)(2,1)S(1)}, bf16[64,256]{1,0:T(8,128)(2,1)}, u32[]{:S(2)}) copy-start(bf16[64,256]{1,0:T(8,128)(2,1)} %param.24) | copy-start | bytes 98308
  48.5 53.8 %copy-start.6 = (f32[256,64]{0,1:T(8,128)S(1)}, f32[256,64]{0,1:T(8,128)}, u32[]{:S(2)}) copy-start(f32[256,64]{0,1:T(8,128)} %param.21) | copy-start | bytes 196612
  49.0 58.6 %copy-start.4 = (bf16[64,256]{1,0:T(8,128)(2,1)S(1)}, bf16[64,256]{1,0:T(8,128)(2,1)}, u32[]{:S(2)}) copy-start(bf16[64,256]{1,0:T(8,128)(2,1)} %param.23) | copy-start | bytes 98308
  49.0 58.6 %copy-start.7 = (f32[64,256]{1,0:T(8,128)S(1)}, f32[64,256]{1,0:T(8,128)}, u32[]{:S(2)}) copy-start(f32[64,256]{1,0:T(8,128)} %param.20) | copy-start | bytes 196612
  49.1 59.3 %copy-start.5 = (bf16[64,256]{1,0:T(8,128)(2,1)S(1)}, bf16[64,256]{1,0:T(8,128)(2,1)}, u32[]{:S(2)}) copy-start(bf16[64,256]{1,0:T(8,128)(2,1)} %param.22) | copy-start | bytes 98308
  49.1 59.3 %copy-start.8 = (f32[64,256]{1,0:T(8,128)S(1)}, f32[64,256]{1,0:T(8,128)}, u32[]{:S(2)}) copy-start(f32[64,256]{1,0:T(8,128)} %param.19) | copy-start | bytes 196612
  49.9 14.2 %all-to-all-start.2 = ((bf16[32,8,768]{2,1,0:T(8,128)(2,1)}), bf16[32,8,768]{2,1,0:T(8,128)(2,1)S(1)}, u32[]{:S(2)}, u32[]{:S(2)}) async-start(bf16[32,8,768]{2,1,0:T(8,128)(2,1)} %pad_maximum_fusion.1), calls=%async_computation.2 | async-start | bytes 786432 | tf_op jit(solution)/shard_map/all_to_all | solution.py:48
  76.2 9.8 %all-to-all-start.4 = ((f32[16,1,1]{2,1,0:T(1,128)}), f32[16,1,1]{2,1,0:T(1,128)S(1)}, u32[]{:S(2)}, u32[]{:S(2)}) async-start(f32[16,1,1]{2,1,0:T(1,128)} %broadcast_in_dim.30), calls=%async_computation.4 | async-start | bytes 16384 | tf_op jit(solution)/shard_map/all_to_all | solution.py:17
  104.0 14.6 %all-to-all-start.8 = ((bf16[16,256,64]{1,2,0:T(8,128)(2,1)}), bf16[16,256,64]{1,2,0:T(8,128)(2,1)S(1)}, u32[]{:S(2)}, u32[]{:S(2)}) async-start(bf16[16,256,64]{1,2,0:T(8,128)(2,1)} %broadcast_in_dim.34), calls=%async_computation.8 | async-start | bytes 1048576 | tf_op jit(solution)/shard_map/all_to_all | solution.py:17
  125.4 20.5 %all-to-all-start.6 = ((bf16[16,64,512]{2,1,0:T(8,128)(2,1)}), bf16[16,64,512]{2,1,0:T(8,128)(2,1)S(1)}, u32[]{:S(2)}, u32[]{:S(2)}) async-start(bf16[16,64,512]{2,1,0:T(8,128)(2,1)} %broadcast_in_dim.32), calls=%async_computation.6 | async-start | bytes 2097152 | tf_op jit(solution)/shard_map/all_to_all | solution.py:17
where the time goes:
time: 156 us; the launch traced here: 155 us
  blocking collectives  44.8 us (29%)
  waiting for transfers between devices  43.5 us (28%)
  starting transfers between devices  23.2 us (15%)
  matrix products  19.4 us (12%)
  local copies, waits for them, and re-layouts  13.8 us (9%)
  other arithmetic  8.29 us (5%)
  between operations  1.75 us (1%)
    all_to_all x5, blocking collectives, copy_for_each(): return lax.all_to_all(copies, axis, split_axis=0, concat_axis=0, tiled=True)  44.8 us
    all_to_all x4, waiting for transfers between devices, copy_for_each(): return lax.all_to_all(copies, axis, split_axis=0, concat_axis=0, tiled=True)  33.3 us
    all_to_all x4, starting transfers between devices, copy_for_each(): return lax.all_to_all(copies, axis, split_axis=0, concat_axis=0, tiled=True)  19.3 us
    all_to_all x1, waiting for transfers between devices, sent_and_summed(): lax.all_to_all(in_blocks(value, dim, devices), axis, 0, 0, tiled=True)  10.2 us
    broadcast_in_dim x9, local copies, waits for them, and re-layouts, copy_for_each(): copies = jnp.broadcast_to(value, (lax.axis_size(axis), *value.shape))  5.9 us
    dot_general x1, matrix products, body(): grad_k = jnp.dot(x_cols, key_cot, preferred_element_type=jnp.float32)  5.9 us
    dot_general x1, matrix products, body(): grad_v = jnp.dot(x_cols, value_cot, preferred_element_type=jnp.float32)  5.9 us
    unnamed x35, local copies, waits for them, and re-layouts  4.84 us
  transfers between devices with their start and end apart: 5, of which 5 were waited for; matrix products, arithmetic and copies ran while one was open for 15% of the time, Pallas kernels for 0%

commit v1 on v0

v1 whole, which is shorter than its diff:
```python
import jax
import jax.numpy as jnp
from jax import lax
from jax.experimental import pallas as pl
from jax.experimental.pallas import tpu as pltpu
from jax.sharding import Mesh
from jax.sharding import PartitionSpec as P

FS = ("fs_0", "fs_1", "fs_2")
BF16, F32 = jnp.bfloat16, jnp.float32
MESH = pl.DeviceIdType.MESH

beta_one = 0.9
beta_two = 0.9
learn_rate = 0.01

N_FS, N_TP = 32, 4
TOKENS, D, RANK, COLS = 2048, 2048, 256, 256
ROWS = D // N_FS
TILES = D // 256
WIDTH = 3 * COLS
AHEAD = 3


def kernel(
    x, h, kc, vc, oc, wk, wv, wo, pk, pv, po, mk, mv, mo,
    step_k, step_v, step_o, copy_k, copy_v, copy_o, new_k, new_v, new_o,
    xbuf, cots, cots_t, grads, p_all, wm_all, wbuf, mbuf, parts, sums, total_buf,
    step_buf, new_buf, copy_buf, copy_t_buf,
    x_sem, cot_sem, p_sem, w_sem, out_sem,
    send_p, recv_p, pair_p, send_w, recv_w, pair_w,
    send_r, recv_r, send_g, recv_g, send_t, recv_t,
):
    z, y, c, t = (lax.axis_index(name) for name in (*FS, "tp"))
    me = (z * 4 + y) * 2 + c

    def device(da, db, core=0):
        zz = lax.rem(z + c * da + (1 - c) * db + 4, 4)
        yy = lax.rem(y + (1 - c) * da + c * db + 4, 4)
        return zz, yy, lax.rem(c + core, 2), t

    def block(da, db):
        zz, yy, cc, _ = device(da, db)
        return (zz * 4 + yy) * 2 + cc

    def remote(src, dst, send, recv, target):
        return pltpu.make_async_remote_copy(
            src_ref=src, dst_ref=dst, send_sem=send, recv_sem=recv,
            device_id=target, device_id_type=MESH,
        )

    barrier = pltpu.get_barrier_semaphore()
    for far in range(1, N_FS):
        other = lax.rem(me + far, N_FS)
        pl.semaphore_signal(
            barrier, inc=1, device_id=(other // 8, lax.rem(other // 2, 4), lax.rem(other, 2), t),
            device_id_type=MESH,
        )
    for far in range(1, N_TP):
        pl.semaphore_signal(
            barrier, inc=1, device_id=(z, y, c, lax.rem(t + far, N_TP)), device_id_type=MESH
        )

    def local(src, dst, sem):
        return pltpu.make_async_copy(src, dst, sem)

    p_in = [
        local(ref, p_all.at[me, :, pl.ds(k * COLS, COLS)], p_sem.at[k])
        for k, ref in enumerate((pk, pv, po))
    ]
    cot_in = [local(ref, cots.at[k], cot_sem.at[k]) for k, ref in enumerate((kc, vc, h))]
    w_in = [local(ref, wbuf.at[k], w_sem.at[k]) for k, ref in enumerate((wk, wv, wo))]
    m_in = [local(ref, mbuf.at[k], w_sem.at[3 + k]) for k, ref in enumerate((mk, mv, mo))]

    def tile_in(n):
        src = x if n < TILES else oc
        col = (n % TILES) * 256
        return local(src.at[:, pl.ds(col, 256)], xbuf.at[n], x_sem.at[n])

    for copy in (*p_in, *cot_in):
        copy.start()
    for n in range(AHEAD):
        tile_in(n).start()
    for copy in (*w_in, *m_in):
        copy.start()

    def transposed(k):
        cot_in[k].wait()
        for part in range(4):
            rows = pl.ds(part * 512, 512)
            cots_t[pl.ds(k * 256, 256), rows] = cots[k, rows, :].T

    def compute(n):
        tile_in(n).wait()
        if n + AHEAD < 2 * TILES:
            tile_in(n + AHEAD).start()
        lower, size = (0, 512) if n < TILES else (512, 256)
        made = jnp.dot(
            cots_t[pl.ds(lower, size), :], xbuf[n], preferred_element_type=F32
        )
        grads[pl.ds(lower, size), pl.ds((n % TILES) * 256, 256)] = made.astype(BF16)

    class Gather:
        def __init__(self, buf, split, send, recv, pair):
            self.buf, self.send, self.recv, self.pair = buf, send, recv, pair
            rows = buf.shape[1]
            self.part = {0: pl.ds(0, rows), 1: pl.ds(0, split), 2: pl.ds(split, rows - split)}
            self.slot = {("a", -1): 0, ("a", 1): 1, ("a2", 1): 2, ("a2", 2): 3}
            for i, da in enumerate((0, -1, 1, 2)):
                for j, key in enumerate((("b", da, -1), ("b", da, 1), ("b2", da, 1), ("b2", da, 2))):
                    self.slot[key] = 4 + 4 * i + j

        def go(self, offset, part, key, target):
            ref = self.buf.at[block(*offset), self.part[part], :]
            remote(ref, ref, self.send, self.recv.at[self.slot[key]], target).start()

        def pair_up(self, offset):
            ref = self.buf.at[block(*offset)]
            remote(ref, ref, self.send, self.pair, device(0, 0, 1)).start()

        def arrived(self, key, offset, part):
            ref = self.buf.at[block(*offset), self.part[part], :]
            remote(ref, ref, self.send, self.recv.at[self.slot[key]], device(0, 0, 1)).wait_recv()

        def both(self, da, offset):
            self.go(offset, 0, ("b", da, -1), device(0, 1))
            self.go(offset, 0, ("b", da, 1), device(0, -1))

        def on_b(self, da, side):
            self.arrived(("b", da, side), (da, side), 0)
            part = 1 if side < 0 else 2
            self.go((da, side), part, ("b2", da, part), device(0, -side))
            self.pair_up((da, side))

        def last_b(self, da):
            for part in (1, 2):
                self.arrived(("b2", da, part), (da, 2), part)
            self.pair_up((da, 2))

        def first(self):
            self.go((0, 0), 0, ("a", -1), device(1, 0))
            self.go((0, 0), 0, ("a", 1), device(-1, 0))
            self.both(0, (0, 0))
            self.pair_up((0, 0))

        def second(self):
            for side in (-1, 1):
                self.arrived(("a", side), (side, 0), 0)
                part = 1 if side < 0 else 2
                self.go((side, 0), part, ("a2", part), device(-side, 0))
            for side in (-1, 1):
                self.both(side, (side, 0))
                self.pair_up((side, 0))
            for side in (-1, 1):
                self.on_b(0, side)

        def third(self):
            for part in (1, 2):
                self.arrived(("a2", part), (2, 0), part)
            self.both(2, (2, 0))
            self.pair_up((2, 0))
            for da in (-1, 1):
                for side in (-1, 1):
                    self.on_b(da, side)
            self.last_b(0)

        def fourth(self):
            for side in (-1, 1):
                self.on_b(2, side)
            for da in (-1, 1):
                self.last_b(da)

        def fifth(self):
            self.last_b(2)

        def done(self):
            half = self.buf.at[pl.ds(0, 16)]
            remote(half, half, self.send, self.pair, device(0, 0, 1)).wait_recv()

        def drained(self):
            most = self.buf.at[pl.ds(0, 31)]
            remote(most, most, self.send, self.pair, device(0, 0, 1)).wait_send()

    factors = Gather(p_all, 32, send_p, recv_p, pair_p)
    states = Gather(wm_all, 48, send_w, recv_w, pair_w)

    transposed(0)
    transposed(1)
    pl.semaphore_wait(barrier, N_FS - 1 + N_TP - 1)
    for copy in p_in:
        copy.wait()
    factors.first()
    for n in range(7):
        compute(n)
    for copy in (*w_in, *m_in):
        copy.wait()
    for k in range(3):
        cols = pl.ds(k * COLS, COLS)
        wm_all[me, pl.ds(0, ROWS), cols] = wbuf[k].astype(BF16)
        wm_all[me, pl.ds(ROWS, 16), cols] = mbuf[k].reshape(16, COLS).astype(BF16)
    factors.second()
    compute(7)
    transposed(2)
    for n in range(TILES, 2 * TILES):
        compute(n)
    factors.third()
    factors.fourth()
    states.first()
    factors.fifth()
    factors.done()

    for k in range(3):
        cols = pl.ds(k * COLS, COLS)
        made = jnp.dot(
            grads[cols, :], p_all[:, :, cols].reshape(D, RANK), preferred_element_type=F32
        ).T
        stacked = jnp.concatenate(
            [made[:, :128].reshape(N_FS, 8, 128), made[:, 128:].reshape(N_FS, 8, 128)], axis=1
        )
        parts[0, :, pl.ds(k * 16, 16), :] = stacked.astype(BF16)

    def to_each(make):
        @pl.loop(1, N_FS)
        def _(far):
            other = lax.rem(me + far, N_FS)
            make(other, (other // 8, lax.rem(other // 2, 4), lax.rem(other, 2), t)).start()

    to_each(lambda other, target: remote(
        parts.at[0, other], parts.at[1, me], send_r, recv_r, target))
    states.second()
    rest = parts.at[1, pl.ds(0, N_FS - 1)]
    remote(rest, rest, send_r, recv_r, device(0, 0, 1)).wait_recv()
    parts[1, me] = parts[0, me]
    owned = jnp.sum(parts[1].astype(F32), axis=0)
    sums[me] = owned.astype(BF16)
    to_each(lambda other, target: remote(sums.at[me], sums.at[me], send_g, recv_g, target))
    states.third()
    rest = sums.at[pl.ds(0, N_FS - 1)]
    remote(rest, rest, send_g, recv_g, device(0, 0, 1)).wait_recv()

    wide = sums[...].astype(F32)
    squares = jnp.sum(jnp.sum((wide * wide).reshape(N_FS, 6, 8, 128), axis=0), axis=0)
    total_buf[t] = squares
    for far in range(1, N_TP):
        remote(
            total_buf.at[t], total_buf.at[t], send_t.at[far - 1], recv_t.at[far - 1],
            (z, y, c, lax.rem(t + far, N_TP)),
        ).start()
    states.fourth()
    for far in range(1, N_TP):
        remote(
            total_buf.at[t], total_buf.at[lax.rem(t + N_TP - far, N_TP)], send_t.at[far - 1],
            recv_t.at[far - 1], (z, y, c, lax.rem(t + far, N_TP)),
        ).wait_recv()
    total = jnp.sum(total_buf[0] + total_buf[1] + total_buf[2] + total_buf[3], keepdims=True)
    scale = 1.0 / jnp.sqrt(total / (3 * RANK * 4 * COLS) + 1e-06)
    states.fifth()

    outs = []
    for k, out in enumerate((new_k, new_v, new_o)):
        piece = owned[k * 16 : (k + 1) * 16]
        normed = jnp.concatenate([piece[:8], piece[8:]], axis=1) * scale
        new_buf[k, 0] = beta_one * mbuf[k, 0] + (1 - beta_one) * normed
        new_buf[k, 1] = beta_two * mbuf[k, 1] + (1 - beta_two) * normed * normed
        outs.append(local(new_buf.at[k], out, out_sem.at[k]))
        outs[-1].start()
    states.done()

    for k in range(3):
        cols = pl.ds(k * COLS, COLS)
        piece = sums[:, pl.ds(k * 16, 16), :].astype(F32)
        normed = jnp.concatenate([piece[:, :8], piece[:, 8:]], axis=2) * scale[:, :, None]
        old = wm_all[:, pl.ds(ROWS, 16), cols].astype(F32)
        moment_one = beta_one * old[:, :8] + (1 - beta_one) * normed
        moment_two = beta_two * old[:, 8:] + (1 - beta_two) * normed * normed
        direction = (moment_one * lax.rsqrt(moment_two)).reshape(RANK, COLS).astype(BF16)
        made = jnp.dot(p_all[me, :, cols], direction, preferred_element_type=F32)
        step_buf[k] = made
        outs.append(local(step_buf.at[k], (step_k, step_v, step_o)[k], out_sem.at[3 + k]))
        outs[-1].start()
        for part in range(4):
            rows = pl.ds(part * 8, 8)
            made = jnp.dot(
                p_all[rows, :, cols].reshape(512, RANK), direction, preferred_element_type=F32
            )
            fresh = wm_all[rows, pl.ds(0, ROWS), cols].reshape(512, COLS).astype(F32)
            fresh = fresh - learn_rate * made
            long = pl.ds(part * 512, 512)
            if k < 2:
                copy_buf[k, long, :] = fresh.astype(BF16)
                src, dst = copy_buf.at[k, long, :], (copy_k, copy_v)[k].at[long, :]
            else:
                copy_t_buf[:, long] = fresh.T.astype(BF16)
                src, dst = copy_t_buf.at[:, long], copy_o.at[:, long]
            outs.append(local(src, dst, out_sem.at[6 + k * 4 + part]))
            outs[-1].start()

    factors.drained()
    states.drained()
    rest = parts.at[0, pl.ds(0, N_FS - 1)]
    remote(rest, rest, send_r, recv_r, device(0, 0, 1)).wait_send()
    rest = sums.at[pl.ds(0, N_FS - 1)]
    remote(rest, rest, send_g, recv_g, device(0, 0, 1)).wait_send()
    for far in range(1, N_TP):
        remote(
            total_buf.at[t], total_buf.at[t], send_t.at[far - 1], recv_t.at[far - 1],
            (z, y, c, lax.rem(t + far, N_TP)),
        ).wait_send()
    for copy in outs:
        copy.wait()


def body(x, h, kc, vc, oc, wk, wv, wo, pk, pv, po, mk, mv, mo):
    anywhere = pl.BlockSpec(memory_space=pl.ANY)
    dma = pltpu.SemaphoreType.DMA
    outs = pl.pallas_call(
        kernel,
        out_shape=[
            *[jax.ShapeDtypeStruct((ROWS, COLS), F32)] * 3,
            *[jax.ShapeDtypeStruct((D, COLS), BF16)] * 2,
            jax.ShapeDtypeStruct((COLS, D), BF16),
            *[jax.ShapeDtypeStruct((2, 8, COLS), F32)] * 3,
        ],
        in_specs=[anywhere] * 14,
        out_specs=[anywhere] * 9,
        scratch_shapes=[
            pltpu.VMEM((2 * TILES, TOKENS, 256), BF16),
            pltpu.VMEM((3, TOKENS, COLS), BF16),
            pltpu.VMEM((WIDTH, TOKENS), BF16),
            pltpu.VMEM((WIDTH, D), BF16),
            pltpu.VMEM((N_FS, ROWS, WIDTH), BF16),
            pltpu.VMEM((N_FS, ROWS + 16, WIDTH), BF16),
            pltpu.VMEM((3, ROWS, COLS), F32),
            pltpu.VMEM((3, 2, 8, COLS), F32),
            pltpu.VMEM((2, N_FS, 48, 128), BF16),
            pltpu.VMEM((N_FS, 48, 128), BF16),
            pltpu.VMEM((N_TP, 8, 128), F32),
            pltpu.VMEM((3, ROWS, COLS), F32),
            pltpu.VMEM((3, 2, 8, COLS), F32),
            pltpu.VMEM((2, D, COLS), BF16),
            pltpu.VMEM((COLS, D), BF16),
            dma((2 * TILES,)), dma((3,)), dma((3,)), dma((6,)), dma((18,)),
            dma, dma((20,)), dma, dma, dma((20,)), dma,
            dma, dma, dma, dma, dma((3,)), dma((3,)),
        ],
        compiler_params=pltpu.CompilerParams(
            collective_id=0, has_side_effects=True, vmem_limit_bytes=60 * 2**20
        ),
    )(x, h, kc, vc, oc, wk, wv, wo.T, pk, pv, po, mk, mv, mo)
    step_k, step_v, step_o, *rest = outs
    return step_k, step_v, step_o.T, *rest


def solution(mesh):
    split = Mesh(mesh.devices.reshape(4, 4, 2, mesh.shape["tp"]), (*FS, "tp"))
    rows, both, cols = P(FS, None), P(FS, "tp"), P("tp", FS)
    moments = P(None, FS, "tp")
    return jax.shard_map(
        body,
        mesh=split,
        in_specs=(rows, both, both, both, rows, both, both, cols, rows, rows, rows, *[moments] * 3),
        out_specs=(
            both, both, cols, P(None, "tp"), P(None, "tp"), P("tp", None), *[moments] * 3
        ),
        check_vma=False,
    )
```

time: 156 us -> 75.1 us (0.48)
  Pallas kernels: 0 us -> 58.7 us
  blocking collectives: 44.8 us -> 0 us
  waiting for transfers between devices: 43.5 us -> 0 us
  starting transfers between devices: 23.2 us -> 0 us
  matrix products: 19.4 us -> 0 us
  other arithmetic: 8.29 us -> 0 us
    pallas_call x0 -> x1, Pallas kernels: none -> 58.7 us  [body(): pl.pallas_call(kernel, out_shape=[*[jax.ShapeDtypeStruct((ROWS, COLS), F3...]
    all_to_all x5 -> x0, blocking collectives: 44.8 us -> none  [copy_for_each(): return lax.all_to_all(copies, axis, split_axis=0, concat_axis=0, tiled=True)]
    all_to_all x5 -> x0, waiting for transfers between devices: 43.5 us -> none  [the longest x4 33.3 us: copy_for_each(): return lax.all_to_all(copies, axis, split_axis=0, concat_axis=0, tiled=True)]
    all_to_all x5 -> x0, starting transfers between devices: 23.2 us -> none  [the longest x4 19.3 us: copy_for_each(): return lax.all_to_all(copies, axis, split_axis=0, concat_axis=0, tiled=True)]
    dot_general x12 -> x0, matrix products: 19.4 us -> none  [the longest x1 5.9 us: body(): grad_k = jnp.dot(x_cols, key_cot, preferred_element_type=jnp.float32)]
    unnamed x35 -> x9, local copies, waits for them, and re-layouts: 4.84 us -> 15.2 us
    broadcast_in_dim x9 -> x0, local copies, waits for them, and re-layouts: 5.9 us -> none  [copy_for_each(): copies = jnp.broadcast_to(value, (lax.axis_size(axis), *value.shape))]
    convert_element_type x3 -> x0, other arithmetic: 4.09 us -> none  [the longest x1 2.08 us: project_rows(): low_part = (grads - high_part.astype(jnp.float32)).astype(jnp.bfloat16)]
  transfers between devices with their start and end apart: 5 -> 0, of which waited for: 5 -> 0; matrix products, arithmetic and copies ran while one was open for 15% -> 0% of each run, Pallas kernels for 0% -> 0%
where the time goes in v1:
time: 75.1 us; the launch traced here: 74.6 us
  Pallas kernels  58.7 us (78%)
  local copies, waits for them, and re-layouts  15.2 us (20%)
    pallas_call x1, Pallas kernels, body(): pl.pallas_call(kernel, out_shape=[*[jax.ShapeDtypeStruct((ROWS, COLS), F3...  58.7 us
    unnamed x9, local copies, waits for them, and re-layouts  15.2 us

profile of v1, /device:TPU:1, one launch (start us, length us, event | category | flops | bytes accessed | tf_op | source)
XLA Modules:
  0.0 74.6 jit_solution(7507279777552350479)
XLA Ops:
  0.6 58.7 %shard_map.205 = (f32[64,256]{1,0:T(8,128)}, f32[64,256]{1,0:T(8,128)}, f32[64,256]{1,0:T(8,128)}, bf16[2048,256]{1,0:T(8,128)(2,1)}, bf16[2048,256]{1,0:T(8,128...) custom-call(bf16[2048,2048]{1,0:T(8,128)(2,1)} %x.1, ...), custom_call_target="tpu_custom_call" | custom-call | tf_op jit(solution)/shard_map/pallas_call | solution.py:316
  59.4 1.5 %copy.32 = f32[64,256]{1,0:T(8,128)} copy(f32[64,256]{1,0:T(8,128)} %get-tuple-element.36) | data formatting | bytes 131072
  60.9 1.5 %copy.33 = f32[64,256]{1,0:T(8,128)} copy(f32[64,256]{1,0:T(8,128)} %get-tuple-element.37) | data formatting | bytes 131072
  62.3 1.5 %copy.34 = f32[256,64]{0,1:T(8,128)} copy(f32[256,64]{0,1:T(8,128)} %bitcast.3) | data formatting | bytes 131072
  63.8 2.3 %copy.35 = bf16[2048,256]{1,0:T(8,128)(2,1)} copy(bf16[2048,256]{1,0:T(8,128)(2,1)} %get-tuple-element.39) | data formatting | bytes 2097152
  66.1 2.3 %copy.36 = bf16[2048,256]{1,0:T(8,128)(2,1)} copy(bf16[2048,256]{1,0:T(8,128)(2,1)} %get-tuple-element.40) | data formatting | bytes 2097152
  68.3 2.3 %copy.37 = bf16[256,2048]{1,0:T(8,128)(2,1)} copy(bf16[256,2048]{1,0:T(8,128)(2,1)} %get-tuple-element.41) | data formatting | bytes 2097152
  70.6 1.3 %copy.38 = f32[2,8,256]{2,1,0:T(8,128)} copy(f32[2,8,256]{2,1,0:T(8,128)} %get-tuple-element.42) | data formatting | bytes 32768
  72.0 1.3 %copy.39 = f32[2,8,256]{2,1,0:T(8,128)} copy(f32[2,8,256]{2,1,0:T(8,128)} %get-tuple-element.43) | data formatting | bytes 32768
  73.3 1.3 %copy.40 = f32[2,8,256]{2,1,0:T(8,128)} copy(f32[2,8,256]{2,1,0:T(8,128)} %get-tuple-element.44) | data formatting | bytes 32768

commit v2 on v1

--- a/solution.py
+++ b/solution.py
@@ -19,14 +19,15 @@
 ROWS = D // N_FS
 TILES = D // 256
 WIDTH = 3 * COLS
-AHEAD = 3
-
-
-def kernel(
+AHEAD = 4
+SLOTS = AHEAD + 1
+
+
+def exchange(
     x, h, kc, vc, oc, wk, wv, wo, pk, pv, po, mk, mv, mo,
-    step_k, step_v, step_o, copy_k, copy_v, copy_o, new_k, new_v, new_o,
-    xbuf, cots, cots_t, grads, p_all, wm_all, wbuf, mbuf, parts, sums, total_buf,
-    step_buf, new_buf, copy_buf, copy_t_buf,
+    p_out, wm_out, sums_out, owned_out, scale_out,
+    p_all, wm_all, sums, owned_buf, scale_buf,
+    xbuf, cots, cots_t, grads, wbuf, mbuf, parts, total_buf,
     x_sem, cot_sem, p_sem, w_sem, out_sem,
     send_p, recv_p, pair_p, send_w, recv_w, pair_w,
     send_r, recv_r, send_g, recv_g, send_t, recv_t,
@@ -75,7 +76,7 @@
     def tile_in(n):
         src = x if n < TILES else oc
         col = (n % TILES) * 256
-        return local(src.at[:, pl.ds(col, 256)], xbuf.at[n], x_sem.at[n])
+        return local(src.at[:, pl.ds(col, 256)], xbuf.at[n % SLOTS], x_sem.at[n % SLOTS])
 
     for copy in (*p_in, *cot_in):
         copy.start()
@@ -96,7 +97,7 @@
             tile_in(n + AHEAD).start()
         lower, size = (0, 512) if n < TILES else (512, 256)
         made = jnp.dot(
-            cots_t[pl.ds(lower, size), :], xbuf[n], preferred_element_type=F32
+            cots_t[pl.ds(lower, size), :], xbuf[n % SLOTS], preferred_element_type=F32
         )
         grads[pl.ds(lower, size), pl.ds((n % TILES) * 256, 256)] = made.astype(BF16)
 
@@ -208,6 +209,8 @@
     states.first()
     factors.fifth()
     factors.done()
+    outs = [local(p_all, p_out, out_sem.at[0])]
+    outs[-1].start()
 
     for k in range(3):
         cols = pl.ds(k * COLS, COLS)
@@ -232,11 +235,15 @@
     remote(rest, rest, send_r, recv_r, device(0, 0, 1)).wait_recv()
     parts[1, me] = parts[0, me]
     owned = jnp.sum(parts[1].astype(F32), axis=0)
+    owned_buf[...] = owned
     sums[me] = owned.astype(BF16)
     to_each(lambda other, target: remote(sums.at[me], sums.at[me], send_g, recv_g, target))
     states.third()
     rest = sums.at[pl.ds(0, N_FS - 1)]
     remote(rest, rest, send_g, recv_g, device(0, 0, 1)).wait_recv()
+    for n, (src, dst) in enumerate(((sums, sums_out), (owned_buf, owned_out))):
+        outs.append(local(src, dst, out_sem.at[1 + n]))
+        outs[-1].start()
 
     wide = sums[...].astype(F32)
     squares = jnp.sum(jnp.sum((wide * wide).reshape(N_FS, 6, 8, 128), axis=0), axis=0)
@@ -253,18 +260,61 @@
             recv_t.at[far - 1], (z, y, c, lax.rem(t + far, N_TP)),
         ).wait_recv()
     total = jnp.sum(total_buf[0] + total_buf[1] + total_buf[2] + total_buf[3], keepdims=True)
-    scale = 1.0 / jnp.sqrt(total / (3 * RANK * 4 * COLS) + 1e-06)
+    scale_buf[...] = jnp.broadcast_to(1.0 / jnp.sqrt(total / (3 * RANK * 4 * COLS) + 1e-06), (8, 128))
+    outs.append(local(scale_buf, scale_out, out_sem.at[3]))
+    outs[-1].start()
     states.fifth()
-
+    states.done()
+    outs.append(local(wm_all, wm_out, out_sem.at[4]))
+    outs[-1].start()
+
+
+    factors.drained()
+    states.drained()
+    rest = parts.at[0, pl.ds(0, N_FS - 1)]
+    remote(rest, rest, send_r, recv_r, device(0, 0, 1)).wait_send()
+    rest = sums.at[pl.ds(0, N_FS - 1)]
+    remote(rest, rest, send_g, recv_g, device(0, 0, 1)).wait_send()
+    for far in range(1, N_TP):
+        remote(
+            total_buf.at[t], total_buf.at[t], send_t.at[far - 1], recv_t.at[far - 1],
+            (z, y, c, lax.rem(t + far, N_TP)),
+        ).wait_send()
+    for copy in outs:
+        copy.wait()
+
+
+def update(
+    p_in, wm_in, sums_in, owned_in, scale_in, mk, mv, mo,
+    step_k, step_v, step_o, copy_k, copy_v, copy_o, new_k, new_v, new_o,
+    p_all, wm_all, sums, owned, scale_buf, mbuf, step_buf, new_buf, copy_buf, copy_t_buf,
+    in_sem, out_sem,
+):
+    z, y, c = (lax.axis_index(name) for name in FS)
+    me = (z * 4 + y) * 2 + c
+    rows_in, states_in = pl.ds(0, ROWS), pl.ds(ROWS, 16)
+    first = [
+        (sums_in, sums), (scale_in, scale_buf), (wm_in.at[:, states_in, :], wm_all.at[:, states_in, :]),
+        (owned_in, owned), *[(ref, mbuf.at[k]) for k, ref in enumerate((mk, mv, mo))],
+    ]
+    for k in range(3):
+        cols = pl.ds(k * COLS, COLS)
+        first.append((p_in.at[:, :, cols], p_all.at[:, :, cols]))
+        first.append((wm_in.at[:, rows_in, cols], wm_all.at[:, rows_in, cols]))
+    loads = [pltpu.make_async_copy(*pair, in_sem.at[n]) for n, pair in enumerate(first)]
+    for copy in loads:
+        copy.start()
+    for copy in loads[:7]:
+        copy.wait()
+    scale = scale_buf[pl.ds(0, 1), pl.ds(0, 1)]
     outs = []
     for k, out in enumerate((new_k, new_v, new_o)):
-        piece = owned[k * 16 : (k + 1) * 16]
+        piece = owned[pl.ds(k * 16, 16), :]
         normed = jnp.concatenate([piece[:8], piece[8:]], axis=1) * scale
         new_buf[k, 0] = beta_one * mbuf[k, 0] + (1 - beta_one) * normed
         new_buf[k, 1] = beta_two * mbuf[k, 1] + (1 - beta_two) * normed * normed
-        outs.append(local(new_buf.at[k], out, out_sem.at[k]))
+        outs.append(pltpu.make_async_copy(new_buf.at[k], out, out_sem.at[k]))
         outs[-1].start()
-    states.done()
 
     for k in range(3):
         cols = pl.ds(k * COLS, COLS)
@@ -274,9 +324,11 @@
         moment_one = beta_one * old[:, :8] + (1 - beta_one) * normed
         moment_two = beta_two * old[:, 8:] + (1 - beta_two) * normed * normed
         direction = (moment_one * lax.rsqrt(moment_two)).reshape(RANK, COLS).astype(BF16)
+        loads[7 + 2 * k].wait()
+        loads[8 + 2 * k].wait()
         made = jnp.dot(p_all[me, :, cols], direction, preferred_element_type=F32)
         step_buf[k] = made
-        outs.append(local(step_buf.at[k], (step_k, step_v, step_o)[k], out_sem.at[3 + k]))
+        outs.append(pltpu.make_async_copy(step_buf.at[k], (step_k, step_v, step_o)[k], out_sem.at[3 + k]))
         outs[-1].start()
         for part in range(4):
             rows = pl.ds(part * 8, 8)
@@ -292,62 +344,74 @@
             else:
                 copy_t_buf[:, long] = fresh.T.astype(BF16)
                 src, dst = copy_t_buf.at[:, long], copy_o.at[:, long]
-            outs.append(local(src, dst, out_sem.at[6 + k * 4 + part]))
+            outs.append(pltpu.make_async_copy(src, dst, out_sem.at[6 + k * 4 + part]))
             outs[-1].start()
 
-    factors.drained()
-    states.drained()
-    rest = parts.at[0, pl.ds(0, N_FS - 1)]
-    remote(rest, rest, send_r, recv_r, device(0, 0, 1)).wait_send()
-    rest = sums.at[pl.ds(0, N_FS - 1)]
-    remote(rest, rest, send_g, recv_g, device(0, 0, 1)).wait_send()
-    for far in range(1, N_TP):
-        remote(
-            total_buf.at[t], total_buf.at[t], send_t.at[far - 1], recv_t.at[far - 1],
-            (z, y, c, lax.rem(t + far, N_TP)),
-        ).wait_send()
     for copy in outs:
         copy.wait()
 
 
 def body(x, h, kc, vc, oc, wk, wv, wo, pk, pv, po, mk, mv, mo):
-    anywhere = pl.BlockSpec(memory_space=pl.ANY)
+    anywhere = pl.BlockSpec(memory_space=pltpu.HBM)
     dma = pltpu.SemaphoreType.DMA
-    outs = pl.pallas_call(
-        kernel,
+    held = pl.pallas_call(
+        exchange,
+        out_shape=[
+            jax.ShapeDtypeStruct((N_FS, ROWS, WIDTH), BF16),
+            jax.ShapeDtypeStruct((N_FS, ROWS + 16, WIDTH), BF16),
+            jax.ShapeDtypeStruct((N_FS, 48, 128), BF16),
+            jax.ShapeDtypeStruct((48, 128), F32),
+            jax.ShapeDtypeStruct((8, 128), F32),
+        ],
+        in_specs=[anywhere] * 14,
+        out_specs=[anywhere] * 5,
+        scratch_shapes=[
+            pltpu.VMEM((N_FS, ROWS, WIDTH), BF16),
+            pltpu.VMEM((N_FS, ROWS + 16, WIDTH), BF16),
+            pltpu.VMEM((N_FS, 48, 128), BF16),
+            pltpu.VMEM((48, 128), F32),
+            pltpu.VMEM((8, 128), F32),
+            pltpu.VMEM((SLOTS, TOKENS, 256), BF16),
+            pltpu.VMEM((3, TOKENS, COLS), BF16),
+            pltpu.VMEM((WIDTH, TOKENS), BF16),
+            pltpu.VMEM((WIDTH, D), BF16),
+            pltpu.VMEM((3, ROWS, COLS), F32),
+            pltpu.VMEM((3, 2, 8, COLS), F32),
+            pltpu.VMEM((2, N_FS, 48, 128), BF16),
+            pltpu.VMEM((N_TP, 8, 128), F32),
+            dma((SLOTS,)), dma((3,)), dma((3,)), dma((6,)), dma((5,)),
+            dma, dma((20,)), dma, dma, dma((20,)), dma,
+            dma, dma, dma, dma, dma((3,)), dma((3,)),
+        ],
+        compiler_params=pltpu.CompilerParams(
+            collective_id=0, has_side_effects=True, vmem_limit_bytes=63 * 2**20
+        ),
+    )(x, h, kc, vc, oc, wk, wv, wo.T, pk, pv, po, mk, mv, mo)
+    step_k, step_v, step_o, *rest = pl.pallas_call(
+        update,
         out_shape=[
             *[jax.ShapeDtypeStruct((ROWS, COLS), F32)] * 3,
             *[jax.ShapeDtypeStruct((D, COLS), BF16)] * 2,
             jax.ShapeDtypeStruct((COLS, D), BF16),
             *[jax.ShapeDtypeStruct((2, 8, COLS), F32)] * 3,
         ],
-        in_specs=[anywhere] * 14,
+        in_specs=[anywhere] * 8,
         out_specs=[anywhere] * 9,
         scratch_shapes=[
-            pltpu.VMEM((2 * TILES, TOKENS, 256), BF16),
-            pltpu.VMEM((3, TOKENS, COLS), BF16),
-            pltpu.VMEM((WIDTH, TOKENS), BF16),
-            pltpu.VMEM((WIDTH, D), BF16),
             pltpu.VMEM((N_FS, ROWS, WIDTH), BF16),
             pltpu.VMEM((N_FS, ROWS + 16, WIDTH), BF16),
-            pltpu.VMEM((3, ROWS, COLS), F32),
+            pltpu.VMEM((N_FS, 48, 128), BF16),
+            pltpu.VMEM((48, 128), F32),
+            pltpu.VMEM((8, 128), F32),
             pltpu.VMEM((3, 2, 8, COLS), F32),
-            pltpu.VMEM((2, N_FS, 48, 128), BF16),
-            pltpu.VMEM((N_FS, 48, 128), BF16),
-            pltpu.VMEM((N_TP, 8, 128), F32),
             pltpu.VMEM((3, ROWS, COLS), F32),
             pltpu.VMEM((3, 2, 8, COLS), F32),
             pltpu.VMEM((2, D, COLS), BF16),
             pltpu.VMEM((COLS, D), BF16),
-            dma((2 * TILES,)), dma((3,)), dma((3,)), dma((6,)), dma((18,)),
-            dma, dma((20,)), dma, dma, dma((20,)), dma,
-            dma, dma, dma, dma, dma((3,)), dma((3,)),
+            dma((13,)), dma((18,)),
         ],
-        compiler_params=pltpu.CompilerParams(
-            collective_id=0, has_side_effects=True, vmem_limit_bytes=60 * 2**20
-        ),
-    )(x, h, kc, vc, oc, wk, wv, wo.T, pk, pv, po, mk, mv, mo)
-    step_k, step_v, step_o, *rest = outs
+        compiler_params=pltpu.CompilerParams(vmem_limit_bytes=63 * 2**20),
+    )(*held, mk, mv, mo)
     return step_k, step_v, step_o.T, *rest
 
 

time: 75.1 us -> 63.6 us (0.85)
  local copies, waits for them, and re-layouts: 15.2 us -> 0 us
  Pallas kernels: 58.7 us -> 62.8 us
    unnamed x9 -> x0, local copies, waits for them, and re-layouts: 15.2 us -> none
    pallas_call x1 -> x2, Pallas kernels: 58.7 us -> 62.8 us  [the longest x1 57.7 us: body(): pl.pallas_call(exchange, out_shape=[jax.ShapeDtypeStruct((N_FS, ROWS, WID...]
where the time goes in v2:
time: 63.6 us; the launch traced here: 63.5 us
  Pallas kernels  62.8 us (99%)
  between operations  0.65 us (1%)
    pallas_call x1, Pallas kernels, body(): pl.pallas_call(exchange, out_shape=[jax.ShapeDtypeStruct((N_FS, ROWS, WID...  57.7 us
    pallas_call x1, Pallas kernels, body(): pl.pallas_call(update, out_shape=[*[jax.ShapeDtypeStruct((ROWS, COLS), F3...  5.11 us

profile of v2, /device:TPU:1, one launch (start us, length us, event | category | flops | bytes accessed | tf_op | source)
XLA Modules:
  0.0 63.5 jit_solution(4432992769481993187)
XLA Ops:
  0.6 57.7 %shard_map.205 = (bf16[32,64,768]{2,1,0:T(8,128)(2,1)}, bf16[32,80,768]{2,1,0:T(8,128)(2,1)}, bf16[32,48,128]{2,1,0:T(8,128)(2,1)}, f32[48,128]{1,0:T(8,128)}, f32[8,128]{1,0:T(8,128)}) custom-call(bf16[2048,2048]{1,0:T(8,128)(2,1)} %x.1, bf16[2048,256]{1,0:T(8,128)(2,1)} %h.1, bf16[2048,256]{1,0:T(8,128)(2,1)} %kc.1, bf16[2048,256]{1,0:T(8,128)(2,1)} %vc.1, ...), custom_call_target="tpu_custom_call" | custom-call | tf_op jit(solution)/shard_map/pallas_call | solution.py:357
  58.4 5.1 %shard_map.206 = (f32[64,256]{1,0:T(8,128)}, f32[64,256]{1,0:T(8,128)}, f32[64,256]{1,0:T(8,128)}, bf16[2048,256]{1,0:T(8,128)(2,1)}, bf16[2048,256]{1,0:T(8,128...) custom-call(bf16[32,64,768]{2,1,0:T(8,128)(2,1)} %get-tuple-element.23.p, ...), custom_call_target="tpu_custom_call" | custom-call | tf_op jit(solution)/shard_map/pallas_call | solution.py:390

commit v3 on v2

v3 whole, which is shorter than its diff:
```python
import jax
import jax.numpy as jnp
from jax import lax
from jax.experimental import pallas as pl
from jax.experimental.pallas import tpu as pltpu
from jax.sharding import Mesh
from jax.sharding import PartitionSpec as P

FS = ("fs_0", "fs_1", "fs_2")
BF16, F32 = jnp.bfloat16, jnp.float32
MESH = pl.DeviceIdType.MESH

beta_one = 0.9
beta_two = 0.9
learn_rate = 0.01

N_FS, N_TP = 32, 4
TOKENS, D, RANK, COLS = 2048, 2048, 256, 256
ROWS = D // N_FS
TILE = 512
TILES = D // TILE
WIDTH = 3 * COLS
AHEAD = 3
SLOTS = AHEAD + 1


def exchange(
    x, h, kc, vc, oc, wk, wv, wo, pk, pv, po, mk, mv, mo,
    p_all, wm_all, sums, owned_buf, scale_buf,
    xbuf, cots, cots_t, grads, wbuf, mbuf, parts, pair_buf, half, ring_a, some, ring_b, total_buf,
    x_sem, cot_sem, p_sem, w_sem,
    send_p, recv_p, pair_p, send_w, recv_w, pair_w, step_send, step_recv,
):
    z, y, c, t = (lax.axis_index(name) for name in (*FS, "tp"))
    me = (z * 4 + y) * 2 + c

    def device(da, db, core=0):
        zz = lax.rem(z + c * da + (1 - c) * db + 4, 4)
        yy = lax.rem(y + (1 - c) * da + c * db + 4, 4)
        return zz, yy, lax.rem(c + core, 2), t

    def block(da, db):
        zz, yy, cc, _ = device(da, db)
        return (zz * 4 + yy) * 2 + cc

    def remote(src, dst, send, recv, target):
        return pltpu.make_async_remote_copy(
            src_ref=src, dst_ref=dst, send_sem=send, recv_sem=recv,
            device_id=target, device_id_type=MESH,
        )

    barrier = pltpu.get_barrier_semaphore()
    for far in range(1, N_FS):
        other = lax.rem(me + far, N_FS)
        pl.semaphore_signal(
            barrier, inc=1, device_id=(other // 8, lax.rem(other // 2, 4), lax.rem(other, 2), t),
            device_id_type=MESH,
        )
    for far in range(1, N_TP):
        for core in range(2):
            pl.semaphore_signal(
                barrier, inc=1, device_id=(z, y, core, lax.rem(t + far, N_TP)), device_id_type=MESH
            )

    def local(src, dst, sem):
        return pltpu.make_async_copy(src, dst, sem)

    p_in = [
        local(ref, p_all.at[me, :, pl.ds(k * COLS, COLS)], p_sem.at[k])
        for k, ref in enumerate((pk, pv, po))
    ]
    cot_in = [local(ref, cots.at[k], cot_sem.at[k]) for k, ref in enumerate((kc, vc, h))]
    w_in = [local(ref, wbuf.at[k], w_sem.at[k]) for k, ref in enumerate((wk, wv, wo))]
    m_in = [local(ref, mbuf.at[k], w_sem.at[3 + k]) for k, ref in enumerate((mk, mv, mo))]

    def tile_in(n):
        src = x if n < TILES else oc
        col = (n % TILES) * TILE
        return local(src.at[:, pl.ds(col, TILE)], xbuf.at[n % SLOTS], x_sem.at[n % SLOTS])

    for copy in (*p_in, *cot_in):
        copy.start()
    for n in range(AHEAD):
        tile_in(n).start()
    for copy in (*w_in, *m_in):
        copy.start()

    def transposed(k):
        cot_in[k].wait()
        for part in range(4):
            rows = pl.ds(part * 512, 512)
            cots_t[pl.ds(k * 256, 256), rows] = cots[k, rows, :].T

    def compute(n):
        tile_in(n).wait()
        if n + AHEAD < 2 * TILES:
            tile_in(n + AHEAD).start()
        lower, size = (0, 512) if n < TILES else (512, 256)
        made = jnp.dot(
            cots_t[pl.ds(lower, size), :], xbuf[n % SLOTS], preferred_element_type=F32
        )
        grads[pl.ds(lower, size), pl.ds((n % TILES) * TILE, TILE)] = made.astype(BF16)

    class Gather:
        def __init__(self, buf, split, send, recv, pair):
            self.buf, self.send, self.recv, self.pair = buf, send, recv, pair
            rows = buf.shape[1]
            self.part = {0: pl.ds(0, rows), 1: pl.ds(0, split), 2: pl.ds(split, rows - split)}
            self.slot = {("a", -1): 0, ("a", 1): 1, ("a2", 1): 2, ("a2", 2): 3}
            for i, da in enumerate((0, -1, 1, 2)):
                for j, key in enumerate((("b", da, -1), ("b", da, 1), ("b2", da, 1), ("b2", da, 2))):
                    self.slot[key] = 4 + 4 * i + j

        def go(self, offset, part, key, target):
            ref = self.buf.at[block(*offset), self.part[part], :]
            remote(ref, ref, self.send, self.recv.at[self.slot[key]], target).start()

        def pair_up(self, offset):
            ref = self.buf.at[block(*offset)]
            remote(ref, ref, self.send, self.pair, device(0, 0, 1)).start()

        def arrived(self, key, offset, part):
            ref = self.buf.at[block(*offset), self.part[part], :]
            remote(ref, ref, self.send, self.recv.at[self.slot[key]], device(0, 0, 1)).wait_recv()

        def both(self, da, offset):
            self.go(offset, 0, ("b", da, -1), device(0, 1))
            self.go(offset, 0, ("b", da, 1), device(0, -1))

        def on_b(self, da, side):
            self.arrived(("b", da, side), (da, side), 0)
            part = 1 if side < 0 else 2
            self.go((da, side), part, ("b2", da, part), device(0, -side))
            self.pair_up((da, side))

        def last_b(self, da):
            for part in (1, 2):
                self.arrived(("b2", da, part), (da, 2), part)
            self.pair_up((da, 2))

        def first(self):
            self.go((0, 0), 0, ("a", -1), device(1, 0))
            self.go((0, 0), 0, ("a", 1), device(-1, 0))
            self.both(0, (0, 0))
            self.pair_up((0, 0))

        def second(self):
            self.second_a()
            self.second_b()
            self.second_c()

        def third(self):
            self.third_a()
            self.third_b()

        def second_a(self):
            for side in (-1, 1):
                self.arrived(("a", side), (side, 0), 0)
                part = 1 if side < 0 else 2
                self.go((side, 0), part, ("a2", part), device(-side, 0))
            self.both(-1, (-1, 0))
            self.pair_up((-1, 0))

        def second_b(self):
            self.both(1, (1, 0))
            self.pair_up((1, 0))

        def second_c(self):
            for side in (-1, 1):
                self.on_b(0, side)

        def third_a(self):
            for part in (1, 2):
                self.arrived(("a2", part), (2, 0), part)
            self.both(2, (2, 0))
            self.pair_up((2, 0))

        def third_b(self):
            for da in (-1, 1):
                for side in (-1, 1):
                    self.on_b(da, side)
            self.last_b(0)

        def fourth(self):
            for side in (-1, 1):
                self.on_b(2, side)
            for da in (-1, 1):
                self.last_b(da)

        def fifth(self):
            self.last_b(2)

        def done(self):
            half = self.buf.at[pl.ds(0, 16)]
            remote(half, half, self.send, self.pair, device(0, 0, 1)).wait_recv()

        def drained(self):
            most = self.buf.at[pl.ds(0, 31)]
            remote(most, most, self.send, self.pair, device(0, 0, 1)).wait_send()

    factors = Gather(p_all, 32, send_p, recv_p, pair_p)
    states = Gather(wm_all, 48, send_w, recv_w, pair_w)

    transposed(0)
    transposed(1)
    pl.semaphore_wait(barrier, N_FS - 1 + 2 * (N_TP - 1))
    for copy in p_in:
        copy.wait()
    factors.first()
    for n in range(TILES):
        compute(n)
    for copy in (*w_in, *m_in):
        copy.wait()
    for k in range(3):
        cols = pl.ds(k * COLS, COLS)
        wm_all[me, pl.ds(0, ROWS), cols] = wbuf[k].astype(BF16)
        wm_all[me, pl.ds(ROWS, 16), cols] = mbuf[k].reshape(16, COLS).astype(BF16)
    factors.second()
    transposed(2)
    for n in range(TILES, 2 * TILES):
        compute(n)
    states.first()
    factors.third()
    factors.fourth()
    factors.fifth()
    factors.done()

    for k in range(3):
        cols = pl.ds(k * COLS, COLS)
        made = jnp.dot(
            grads[cols, :], p_all[:, :, cols].reshape(D, RANK), preferred_element_type=F32
        ).T
        left, right = (
            made[:, lane : lane + 128].reshape(16, 2, 8, 128) for lane in (0, 128)
        )
        stacked = jnp.concatenate([left, right], axis=2).astype(BF16)
        for core in range(2):
            parts[core, :, pl.ds(k * 16, 16), :] = stacked[:, core]

    def exchange_step(n, pairs):
        for src, dst, target in pairs:
            remote(src, dst, step_send.at[n], step_recv.at[n], target).start()

    def step_wait(n, like):
        remote(like, like, step_send.at[n], step_recv.at[n], device(0, 0, 1)).wait_recv()

    def step_sent(n, like):
        remote(like, like, step_send.at[n], step_recv.at[n], device(0, 0, 1)).wait_send()

    place_a, place_b = c * z + (1 - c) * y, c * y + (1 - c) * z

    def owner(pa, pb):
        return (c * pa + (1 - c) * pb) * 4 + c * pb + (1 - c) * pa

    near = lax.rem(c + 1, 2)
    exchange_step(0, [(parts.at[near], pair_buf, device(0, 0, 1))])
    states.second_a()
    step_wait(0, pair_buf)
    half[...] = (parts[c].astype(F32) + pair_buf[...].astype(F32)).astype(BF16)
    for far in range(1, 4):
        there = lax.rem(place_a + far, 4)
        exchange_step(1, [
            (half.at[owner(there, pb)], ring_a.at[far - 1, pb], device(far, 0)) for pb in range(4)
        ])
    states.second_b()
    step_wait(1, ring_a)
    for pb in range(4):
        some[pb] = (
            half[owner(place_a, pb)].astype(F32) + jnp.sum(ring_a[:, pb].astype(F32), axis=0)
        ).astype(BF16)
    exchange_step(2, [
        (some.at[lax.rem(place_b + far, 4)], ring_b.at[far - 1], device(0, far))
        for far in range(1, 4)
    ])
    states.second_c()
    step_wait(2, ring_b)
    owned = some[place_b].astype(F32) + jnp.sum(ring_b[...].astype(F32), axis=0)
    owned_buf[...] = owned
    mine = sums.at[c, owner(place_a, place_b)]
    mine[...] = owned.astype(BF16)
    exchange_step(3, [(mine, mine, device(far, 0)) for far in range(1, 4)])
    states.third_a()
    step_wait(3, ring_b)
    for far in range(1, 4):
        exchange_step(4, [
            (sums.at[c, owner(pa, place_b)], sums.at[c, owner(pa, place_b)], device(0, far))
            for pa in range(4)
        ])
    states.third_b()
    step_wait(4, ring_a)
    exchange_step(5, [(sums.at[c], sums.at[c], device(0, 0, 1))])

    wide = sums[c].astype(F32)
    place_t = c * N_TP + t
    total_buf[place_t] = jnp.sum(jnp.sum((wide * wide).reshape(16, 6, 8, 128), axis=0), axis=0)
    for far in range(1, 2 * N_TP):
        there = lax.rem(place_t + far, 2 * N_TP)
        exchange_step(6, [
            (total_buf.at[place_t], total_buf.at[place_t], (z, y, there // N_TP, lax.rem(there, N_TP)))
        ])
    states.fourth()
    step_wait(6, total_buf.at[pl.ds(0, 2 * N_TP - 1)])
    total = jnp.sum(jnp.sum(total_buf[...], axis=0), keepdims=True)
    scale_buf[...] = jnp.broadcast_to(
        1.0 / jnp.sqrt(total / (3 * RANK * N_TP * COLS) + 1e-06), (8, 128)
    )
    step_wait(5, pair_buf)
    states.fifth()
    states.done()

    factors.drained()
    states.drained()
    step_sent(0, pair_buf)
    step_sent(1, ring_a)
    step_sent(2, ring_b)
    step_sent(3, ring_b)
    step_sent(4, ring_a)
    step_sent(5, pair_buf)
    step_sent(6, total_buf.at[pl.ds(0, 2 * N_TP - 1)])


def update(
    p_all, wm_all, sums, owned, scale_buf, mk, mv, mo,
    step_k, step_v, step_o, copy_k, copy_v, copy_o, new_k, new_v, new_o,
    step_buf, new_buf, copy_buf, copy_t_buf, out_sem,
):
    z, y, c = (lax.axis_index(name) for name in FS)
    me = (z * 4 + y) * 2 + c
    mbuf = (mk, mv, mo)
    scale = scale_buf[pl.ds(0, 1), pl.ds(0, 1)]
    outs = []
    for k, out in enumerate((new_k, new_v, new_o)):
        piece = owned[pl.ds(k * 16, 16), :]
        normed = jnp.concatenate([piece[:8], piece[8:]], axis=1) * scale
        new_buf[k, 0] = beta_one * mbuf[k][0] + (1 - beta_one) * normed
        new_buf[k, 1] = beta_two * mbuf[k][1] + (1 - beta_two) * normed * normed
        outs.append(pltpu.make_async_copy(new_buf.at[k], out, out_sem.at[k]))
        outs[-1].start()

    for k in range(3):
        cols = pl.ds(k * COLS, COLS)
        piece = sums[:, :, pl.ds(k * 16, 16), :].astype(F32)
        piece = jnp.stack([piece[0], piece[1]], axis=1).reshape(N_FS, 16, 128)
        normed = jnp.concatenate([piece[:, :8], piece[:, 8:]], axis=2) * scale[:, :, None]
        old = wm_all[:, pl.ds(ROWS, 16), cols].astype(F32)
        moment_one = beta_one * old[:, :8] + (1 - beta_one) * normed
        moment_two = beta_two * old[:, 8:] + (1 - beta_two) * normed * normed
        direction = (moment_one * lax.rsqrt(moment_two)).reshape(RANK, COLS).astype(BF16)
        made = jnp.dot(p_all[me, :, cols], direction, preferred_element_type=F32)
        step_buf[k] = made
        outs.append(pltpu.make_async_copy(step_buf.at[k], (step_k, step_v, step_o)[k], out_sem.at[3 + k]))
        outs[-1].start()
        for part in range(4):
            rows = pl.ds(part * 8, 8)
            made = jnp.dot(
                p_all[rows, :, cols].reshape(512, RANK), direction, preferred_element_type=F32
            )
            fresh = wm_all[rows, pl.ds(0, ROWS), cols].reshape(512, COLS).astype(F32)
            fresh = fresh - learn_rate * made
            long = pl.ds(part * 512, 512)
            if k < 2:
                copy_buf[k, long, :] = fresh.astype(BF16)
                src, dst = copy_buf.at[k, long, :], (copy_k, copy_v)[k].at[long, :]
            else:
                copy_t_buf[:, long] = fresh.T.astype(BF16)
                src, dst = copy_t_buf.at[:, long], copy_o.at[:, long]
            outs.append(pltpu.make_async_copy(src, dst, out_sem.at[6 + k * 4 + part]))
            outs[-1].start()

    for copy in outs:
        copy.wait()


def body(x, h, kc, vc, oc, wk, wv, wo, pk, pv, po, mk, mv, mo):
    outside = pl.BlockSpec(memory_space=pltpu.HBM)
    inside = pl.BlockSpec(memory_space=pltpu.VMEM)
    dma = pltpu.SemaphoreType.DMA
    args = (x, h, kc, vc, oc, wk, wv, wo.T, pk, pv, po, mk, mv, mo)
    held = pl.pallas_call(
        exchange,
        out_shape=[
            pltpu.VMEM((N_FS, ROWS, WIDTH), BF16),
            pltpu.VMEM((N_FS, ROWS + 16, WIDTH), BF16),
            pltpu.VMEM((2, 16, 48, 128), BF16),
            pltpu.VMEM((48, 128), F32),
            pltpu.VMEM((8, 128), F32),
        ],
        in_specs=[outside] * 14,
        out_specs=[inside] * 5,
        scratch_shapes=[
            pltpu.VMEM((SLOTS, TOKENS, TILE), BF16),
            pltpu.VMEM((3, TOKENS, COLS), BF16),
            pltpu.VMEM((WIDTH, TOKENS), BF16),
            pltpu.VMEM((WIDTH, D), BF16),
            pltpu.VMEM((3, ROWS, COLS), F32),
            pltpu.VMEM((3, 2, 8, COLS), F32),
            pltpu.VMEM((2, 16, 48, 128), BF16),
            pltpu.VMEM((16, 48, 128), BF16),
            pltpu.VMEM((16, 48, 128), BF16),
            pltpu.VMEM((3, 4, 48, 128), BF16),
            pltpu.VMEM((4, 48, 128), BF16),
            pltpu.VMEM((3, 48, 128), BF16),
            pltpu.VMEM((2 * N_TP, 8, 128), F32),
            dma((SLOTS,)), dma((3,)), dma((3,)), dma((6,)),
            dma, dma((20,)), dma, dma, dma((20,)), dma, dma((7,)), dma((7,)),
        ],
        compiler_params=pltpu.CompilerParams(
            collective_id=0, has_side_effects=True, vmem_limit_bytes=42 * 2**20
        ),
    )(*(pltpu.with_memory_space_constraint(arg, pltpu.HBM) for arg in args))
    step_k, step_v, step_o, *rest = pl.pallas_call(
        update,
        out_shape=[
            *[jax.ShapeDtypeStruct((ROWS, COLS), F32)] * 3,
            *[jax.ShapeDtypeStruct((D, COLS), BF16)] * 2,
            jax.ShapeDtypeStruct((COLS, D), BF16),
            *[jax.ShapeDtypeStruct((2, 8, COLS), F32)] * 3,
        ],
        in_specs=[inside] * 8,
        out_specs=[outside] * 9,
        scratch_shapes=[
            pltpu.VMEM((3, ROWS, COLS), F32),
            pltpu.VMEM((3, 2, 8, COLS), F32),
            pltpu.VMEM((2, D, COLS), BF16),
            pltpu.VMEM((COLS, D), BF16),
            dma((18,)),
        ],
        compiler_params=pltpu.CompilerParams(vmem_limit_bytes=42 * 2**20),
    )(*held, mk, mv, mo)
    return step_k, step_v, step_o.T, *rest


def solution(mesh):
    split = Mesh(mesh.devices.reshape(4, 4, 2, mesh.shape["tp"]), (*FS, "tp"))
    rows, both, cols = P(FS, None), P(FS, "tp"), P("tp", FS)
    moments = P(None, FS, "tp")
    return jax.shard_map(
        body,
        mesh=split,
        in_specs=(rows, both, both, both, rows, both, both, cols, rows, rows, rows, *[moments] * 3),
        out_specs=(
            both, both, cols, P(None, "tp"), P(None, "tp"), P("tp", None), *[moments] * 3
        ),
        check_vma=False,
    )
```

time: 63.6 us -> 57 us (0.90)
  Pallas kernels: 62.8 us -> 56.2 us
    pallas_call x1, Pallas kernels: 57.7 us -> 53.7 us  [body(): pl.pallas_call(exchange, out_shape=[pltpu.VMEM((N_FS, ROWS, WIDTH), BF16)...]
    pallas_call x1, Pallas kernels: 5.11 us -> 2.51 us  [body(): pl.pallas_call(update, out_shape=[*[jax.ShapeDtypeStruct((ROWS, COLS), F3...]
where the time goes in v3:
time: 57 us; the launch traced here: 56.9 us
  Pallas kernels  56.2 us (99%)
  between operations  0.7 us (1%)
    pallas_call x1, Pallas kernels, body(): pl.pallas_call(exchange, out_shape=[pltpu.VMEM((N_FS, ROWS, WIDTH), BF16)...  53.7 us
    pallas_call x1, Pallas kernels, body(): pl.pallas_call(update, out_shape=[*[jax.ShapeDtypeStruct((ROWS, COLS), F3...  2.51 us

profile of v3, /device:TPU:1, one launch (start us, length us, event | category | flops | bytes accessed | tf_op | source)
XLA Modules:
  0.0 56.9 jit_solution(15308687007789683534)
XLA Ops:
  0.6 0.0 copy-start
  0.7 0.0 copy-start.1
  0.7 0.0 copy-start.2
  0.7 53.7 %shard_map.205 = (bf16[32,64,768]{2,1,0:T(8,128)(2,1)S(1)}, bf16[32,80,768]{2,1,0:T(8,128)(2,1)S(1)}, bf16[2,16,48,128]{3,2,1,0:T(8,128)(2,1)S(1)}, f32[48,128]{1,0:T(8,128)S(1)}, f32[8,128]{1,0:T(8,128)S(1)}) custom-call(bf16[2048,2048]{1,0:T(8,128)(2,1)} %x.1, bf16[2048,256]{1,0:T(8,128)(2,1)} %h.1, bf16[2048,256]{1,0:T(8,128)(2,1)} %kc.1, ...), custom_call_target="tpu_custom_call" | custom-call | tf_op jit(solution)/shard_map/pallas_call | solution.py:379
  54.4 0.0 copy-done
  54.4 0.0 copy-done.1
  54.4 0.0 copy-done.2
  54.4 2.5 %shard_map.206 = (f32[64,256]{1,0:T(8,128)}, f32[64,256]{1,0:T(8,128)}, f32[64,256]{1,0:T(8,128)}, bf16[2048,256]{1,0:T(8,128)(2,1)}, bf16[2048,256]{1,0:T(8,128...) custom-call(bf16[32,64,768]{2,1,0:T(8,128)(2,1)S(1)} %get-tuple-element., ...), custom_call_target="tpu_custom_call" | custom-call | tf_op jit(solution)/shard_map/pallas_call | solution.py:411
Async XLA Ops:
  0.6 53.7 %copy-start = (f32[2,8,256]{2,1,0:T(8,128)S(1)}, f32[2,8,256]{2,1,0:T(8,128)}, u32[]{:S(2)}) copy-start(f32[2,8,256]{2,1,0:T(8,128)} %mk.3) | copy-start | bytes 49156
  0.7 53.7 %copy-start.1 = (f32[2,8,256]{2,1,0:T(8,128)S(1)}, f32[2,8,256]{2,1,0:T(8,128)}, u32[]{:S(2)}) copy-start(f32[2,8,256]{2,1,0:T(8,128)} %mv.3) | copy-start | bytes 49156
  0.7 53.7 %copy-start.2 = (f32[2,8,256]{2,1,0:T(8,128)S(1)}, f32[2,8,256]{2,1,0:T(8,128)}, u32[]{:S(2)}) copy-start(f32[2,8,256]{2,1,0:T(8,128)} %mo.3) | copy-start | bytes 49156
